TPU v7x, 32 devices: a whole 2x2x4 slice. The times are simulated.
32 devices in a mesh: ep: 4 (over y, x), tp: 8 (over z, core).
Axes of the slice: x: 2, y: 2, z: 4, core: 2. Of those that a mesh axis runs over, the one named last changes fastest.
Arguments:
- queries: bfloat16 [2048, 16, 128], P('ep', 'tp'), may hold values from -125 to 125
- keys: bfloat16 [2048, 16, 128], P('ep', 'tp'), may hold values from -9 to 9
- values: bfloat16 [2048, 16, 128], P('ep', 'tp'), may hold values from -6 to 6
- mixing: float32 [16], P('tp'), may hold values from 0.3 to 0.8
- head_gain: float32 [128], replicated, may hold values from 0.1 to 1.9
- out_weight: bfloat16 [16, 128, 2048], P('tp'), may hold values from -0.125 to 0.125
- tokens_b: bfloat16 [4096, 2048], P(('ep', 'tp')), may hold values from -6 to 6
- norm_gain: float32 [2048], replicated, may hold values from 0.1 to 1.9
- expert_ids: int32 [4096, 2], P(('ep', 'tp')), may hold values from 0 to 3, all different within a row; in each aligned block of 128 rows (0 to 127, 128 to 255, ...) at most 96 rows name the same one
- group_gate: float32 [4096], P(('ep', 'tp')), may hold values from 0.2 to 1
- expert_gate: float32 [4096, 2], P(('ep', 'tp')), may hold values from 0.1 to 0.9
- gate_weight: bfloat16 [4, 2048, 1024], P('ep', None, 'tp'), may hold values from -0.125 to 0.125
- up_weight: bfloat16 [4, 2048, 1024], P('ep', None, 'tp'), may hold values from -0.125 to 0.125
- down_weight: bfloat16 [4, 2048, 1024], P('ep', None, 'tp'), may hold values from -0.1875 to 0.1875
Outputs:
- mixed: bfloat16 [2048, 2048], P(('ep', 'tp'))
- routed: bfloat16 [4096, 2048], P(('ep', 'tp'))
Inputs may be any that keep to these rules, and one draw needn't show every extreme that they name: `expert_ids`: within each aligned block of 128 rows, no expert is named by more than 96 rows, and some block has an expert named by exactly 96 rows.
All inputs are finite; a program needn't handle non-finite values.
Results may differ from a plain program's by a relative error of at most 0.019.
Values may be sent and summed in bfloat16 or wider, within the bound.
A program may use at most 192 MiB of HBM per device.

v0:
```python
import math
import jax
import jax.numpy as jnp
from jax import lax
from jax.sharding import PartitionSpec as P

HEAD = 64


def attend_heads(queries, keys, values, mixing, head_gain):
    shard_rows = queries.shape[0]
    head_count = queries.shape[1]
    value_width = values.shape[2]
    query_start = lax.axis_index("ep") * shard_rows
    score_scale = 1.0 / math.sqrt(HEAD)
    query_pos = query_start + lax.iota(jnp.int32, shard_rows)

    def update(running, key_block, value_block, block_start):
        key_pos = block_start + lax.iota(jnp.int32, shard_rows)
        allowed = key_pos[None, :] <= query_pos[:, None]
        fresh = []
        for map_index in range(2):
            maximum, row_sum, numerator = running[3 * map_index : 3 * map_index + 3]
            offset = map_index * HEAD
            scores = (
                jnp.einsum(
                    "qhd,khd->hqk",
                    queries[:, :, offset : offset + HEAD],
                    key_block[:, :, offset : offset + HEAD],
                    preferred_element_type=jnp.float32,
                )
                * score_scale
            )
            scores = jnp.where(allowed[None], scores, -1e30)
            newmax = jnp.maximum(maximum, jnp.max(scores, axis=2))
            shrink = jnp.exp(maximum - newmax)
            weights = jnp.exp(scores - newmax[:, :, None])
            row_sum = row_sum * shrink + jnp.sum(weights, axis=2)
            numerator = numerator * shrink[:, :, None] + jnp.einsum(
                "hqk,khe->hqe",
                weights.astype(jnp.bfloat16),
                value_block,
                preferred_element_type=jnp.float32,
            )
            fresh += [newmax, row_sum, numerator]
        return tuple(fresh)

    floor_max = jnp.full((head_count, shard_rows), -1e30, jnp.float32)
    zero_sum = jnp.zeros((head_count, shard_rows), jnp.float32)
    zero_acc = jnp.zeros((head_count, shard_rows, value_width), jnp.float32)
    start_state = (floor_max, zero_sum, zero_acc, floor_max, zero_sum, zero_acc)
    running = start_state
    key_piece = lax.all_gather(keys, "ep", axis=0, tiled=True)
    value_piece = lax.all_gather(values, "ep", axis=0, tiled=True)
    blocks = key_piece.shape[0] // shard_rows
    key_blocks = key_piece.reshape(blocks, shard_rows, head_count, key_piece.shape[2])
    value_blocks = value_piece.reshape(blocks, shard_rows, head_count, value_width)

    def visit_block(state, inputs):
        key_block, value_block, block_index = inputs
        block_start = block_index * shard_rows
        state = lax.cond(
            block_start <= query_start + shard_rows - 1,
            lambda state_in: update(state_in, key_block, value_block, block_start),
            lambda state_in: state_in,
            state,
        )
        return (state, None)

    running, unused = lax.scan(
        visit_block, running, (key_blocks, value_blocks, lax.iota(jnp.int32, blocks))
    )
    state = running
    diff = state[2] / state[1][:, :, None] - mixing[:, None, None] * state[5] / state[4][:, :, None]
    normed = diff * lax.rsqrt(jnp.mean(diff * diff, axis=2, keepdims=True) + 1e-05) * head_gain
    return normed.astype(jnp.bfloat16)


def mixer_half(queries, keys, values, mixing, head_gain, out_weight):
    attended = attend_heads(queries, keys, values, mixing, head_gain)
    return lax.psum_scatter(
        jnp.einsum("hqe,hed->qd", attended, out_weight, preferred_element_type=jnp.float32).astype(
            jnp.bfloat16
        ),
        "tp",
        scatter_dimension=0,
        tiled=True,
    )


def expert_half(
    tokens_b, norm_gain, expert_ids, group_gate, expert_gate, gate_weight, up_weight, down_weight
):
    local_rows = tokens_b.shape[0]
    width = tokens_b.shape[1]
    top_count = expert_ids.shape[1]
    ep_count = lax.axis_size("ep")
    local_count = gate_weight.shape[0]
    expert_total = ep_count * local_count
    capacity = 3 * local_rows * top_count // (2 * expert_total)
    tokens_f = tokens_b.astype(jnp.float32)
    normed = (
        tokens_f
        * lax.rsqrt(jnp.mean(tokens_f * tokens_f, axis=1, keepdims=True) + 1e-06)
        * norm_gain
    ).astype(jnp.bfloat16)
    flat_ids = expert_ids.reshape(-1)
    one_hot = (flat_ids[:, None] == lax.iota(jnp.int32, expert_total)[None, :]).astype(jnp.int32)
    slot_rank = jnp.sum((jnp.cumsum(one_hot, axis=0) - one_hot) * one_hot, axis=1)
    slot_index = flat_ids * capacity + slot_rank
    owners = jnp.full((expert_total * capacity,), local_rows, jnp.int32)
    owners = owners.at[slot_index].set(lax.iota(jnp.int32, local_rows * top_count) // top_count)
    padded = jnp.concatenate([normed, jnp.zeros((1, width), jnp.bfloat16)], axis=0)
    outgoing = padded[owners].reshape(ep_count, local_count * capacity, width)
    incoming = lax.all_to_all(outgoing, "ep", split_axis=0, concat_axis=0, tiled=True)
    expert_rows = jnp.transpose(
        incoming.reshape(ep_count, local_count, capacity, width), (1, 0, 2, 3)
    )
    expert_rows = expert_rows.reshape(local_count, ep_count * capacity, width)
    piece_gate = lax.all_gather(gate_weight, "tp", axis=2, tiled=True)
    piece_up = lax.all_gather(up_weight, "tp", axis=2, tiled=True)
    piece_down = lax.all_gather(down_weight, "tp", axis=2, tiled=True)
    gate_part = jnp.einsum(
        "jrd,jdf->jrf", expert_rows, piece_gate, preferred_element_type=jnp.float32
    )
    up_part = jnp.einsum("jrd,jdf->jrf", expert_rows, piece_up, preferred_element_type=jnp.float32)
    hidden = (jax.nn.silu(gate_part) * up_part).astype(jnp.bfloat16)
    expert_out = jnp.einsum(
        "jrf,jdf->jrd", hidden, piece_down, preferred_element_type=jnp.float32
    ).astype(jnp.bfloat16)
    outbound = jnp.transpose(
        expert_out.reshape(local_count, ep_count, capacity, width), (1, 0, 2, 3)
    )
    outbound = outbound.reshape(ep_count, local_count * capacity, width)
    returned = lax.all_to_all(outbound, "ep", split_axis=0, concat_axis=0, tiled=True).reshape(
        expert_total * capacity, width
    )
    picked = returned[slot_index].reshape(local_rows, top_count, width).astype(jnp.float32)
    route_weight = group_gate[:, None] * expert_gate
    return jnp.sum(route_weight[:, :, None] * picked, axis=1).astype(jnp.bfloat16)


def per_device(
    queries,
    keys,
    values,
    mixing,
    head_gain,
    out_weight,
    tokens_b,
    norm_gain,
    expert_ids,
    group_gate,
    expert_gate,
    gate_weight,
    up_weight,
    down_weight,
):
    mixed = mixer_half(queries, keys, values, mixing, head_gain, out_weight)
    routed = expert_half(
        tokens_b,
        norm_gain,
        expert_ids,
        group_gate,
        expert_gate,
        gate_weight,
        up_weight,
        down_weight,
    )
    return (mixed, routed)


def solution(mesh):
    placed = (
        P("ep", "tp", None),
        P("ep", "tp", None),
        P("ep", "tp", None),
        P("tp"),
        P(),
        P("tp", None, None),
        P(("ep", "tp"), None),
        P(),
        P(("ep", "tp"), None),
        P(("ep", "tp")),
        P(("ep", "tp"), None),
        P("ep", None, "tp"),
        P("ep", None, "tp"),
        P("ep", None, "tp"),
    )
    return jax.shard_map(
        per_device,
        mesh=mesh,
        in_specs=placed,
        out_specs=(P(("ep", "tp"), None), P(("ep", "tp"), None)),
        check_vma=False,
    )
```

profile of v0, /device:TPU:0, one launch (start us, length us, event | category | flops | bytes accessed | tf_op | source)
XLA Modules:
  0.0 260.2 jit_solution(6079203360803837472)
XLA Ops:
  7.3 1.8 copy.24
  9.1 1.7 copy.25
  13.4 1.2 reduce-window.6
  15.3 1.4 scatter_custom_fusion
  17.0 1.0 fusion.33
  17.9 21.8 %all-gather.6.cloned.1.call-done = bf16[2048,2,128]{2,0,1:T(8,128)(2,1)} async-done(((bf16[512,2,128]{2,0,1:T(8,128)(2,1)}), bf16[2048,2,128]{2,0,1:T(8,128)(2,1)}) %all-gather.6.cloned.1.call-update) | async-done | bytes 1048592 | tf_op jit(solution)/shard_map/all_gather | solution.py:53
  39.7 2.3 copy.26
  42.0 26.1 %all-gather.8.cloned.1.call-done = bf16[2048,2,128]{2,0,1:T(8,128)(2,1)} async-done(((bf16[512,2,128]{2,0,1:T(8,128)(2,1)}), bf16[2048,2,128]{2,0,1:T(8,128)(2,1)}) %all-gather.8.cloned.1.call-update) | async-done | bytes 1048592 | tf_op jit(solution)/shard_map/all_gather | solution.py:54
  68.1 1.3 copy.28
  69.5 9.8 %while.23 = (s32[]{:T(128)}, f32[2,512]{1,0:T(2,128)S(1)}, f32[2,512]{1,0:T(2,128)S(1)}, f32[2,512,128]{2,1,0:T(8,128)S(1)}, f32[2,512]{1,0:T(2,128)S(1)}, /*ind...) while((s32[]{:T(128)}, f32[2,512]{1,0:T(2,128)S(1)}, ...), condition=%wide.region_7.8_spmd.clone, body=%wide.region_0.7_spmd.clone.sunk | while | flops 410784768 | bytes 17183128 | solution.py:70
  70.8 4.6 %conditional.3 = ((f32[2,512]{1,0:T(2,128)S(1)}, f32[2,512]{1,0:T(2,128)S(1)}, f32[2,512,128]{2,1,0:T(8,128)S(1)}, f32[2,512]{1,0:T(2,128)S(1)}, f32[2,512]{1,0:T(2,128)S(1)}, /*index=5*/f32[2,512,128]{2,1,0:T(8,128)S(1)})) conditional(s32[]{:T(128)} %convert_element_type.87, (f32[2,512]{1,0:T(2,128)S(1)}, f32[2,512]{1,0:T(2,128)S(1)}, ...), branch_computations={%region_1.1_spmd, %region_2.6_spmd} | conditional | flops 410784768 | bytes 17180748 | solution.py:62
  70.8 1.0 dynamic-slice_bitcast_fusion
  79.9 2.1 bitcast_convert_fusion
  82.2 2.5 gather_fusion
  84.6 36.1 %all_to_all.10 = bf16[4,96,2048]{2,1,0:T(8,128)(2,1)} all-to-all(bf16[4,96,2048]{2,1,0:T(8,128)(2,1)S(1)} %bitcast.62), channel_id=1, replica_groups=mesh['ep'=4,'tp'=8] {'ep'}, dimensions={0} | all-to-all | bytes 3145728 | tf_op jit(solution)/shard_map/all_to_all | solution.py:115
  120.7 5.7 %fusion.24 = f32[384,1024]{1,0:T(8,128)} fusion(bf16[384,2048]{1,0:T(8,128)(2,1)} %bitcast.63, bf16[1,2048,1024]{2,1,0:T(8,128)(2,1)} %all-gather.10.cloned.1.call-done), kind=kOutput, calls=%fused_computation.38 | convolution fusion | flops 1610612736 | bytes 7340032 | tf_op jit(solution)/shard_map/jrd,jdf->jrf/dot_general | solution.py:123
  126.4 38.6 %all-gather.12.cloned.1.call-done = bf16[1,2048,1024]{2,1,0:T(8,128)(2,1)} async-done(((bf16[1,2048,128]{2,1,0:T(8,128)(2,1)}), bf16[1,2048,1024]{2,1,0:T(8,128)(2,1)}) %all-gather.12.cloned.1.call-update) | async-done | bytes 4194320 | tf_op jit(solution)/shard_map/all_gather | solution.py:121
  165.0 47.5 %all-gather.14.cloned.1.call-done = bf16[1,2048,1024]{2,1,0:T(8,128)(2,1)} async-done(((bf16[1,2048,128]{2,1,0:T(8,128)(2,1)}), bf16[1,2048,1024]{2,1,0:T(8,128)(2,1)}) %all-gather.14.cloned.1.call-update) | async-done | bytes 4194320 | tf_op jit(solution)/shard_map/all_gather | solution.py:122
  212.5 8.6 %fusion.26 = bf16[384,2048]{1,0:T(8,128)(2,1)} fusion(bf16[1,2048,1024]{2,1,0:T(8,128)(2,1)} %all-gather.14.cloned.1.call-done, f32[384,1024]{1,0:T(8,128)} %fusion.24, bf16[384,2048]{1,0:T(8,128)(2,1)S(1)} %bitcast.64, bf16[1,2048,1024]{2,1,0:T(8,128)(2,1)} %all-gather.12.cloned.1.call-done), kind=kOutput, calls=%fused_computation.41 | convolution fusion | flops 3224371200 | bytes 13107200 | tf_op jit(solution)/shard_map/jrf,jdf->jrd/dot_general | solution.py:128
  221.1 3.8 %all-to-all-start.1 = ((bf16[4,96,2048]{2,1,0:T(8,128)(2,1)}), bf16[4,96,2048]{2,1,0:T(8,128)(2,1)S(1)}, u32[]{:S(2)}, u32[]{:S(2)}) async-start(bf16[4,96,2048]{2,1,0:T(8,128)(2,1)} %bitcast.65), calls=%async_computation.2 | async-start | bytes 3145728 | tf_op jit(solution)/shard_map/all_to_all | solution.py:135
  225.0 19.7 %all-to-all-done.1 = bf16[4,96,2048]{2,1,0:T(8,128)(2,1)S(1)} async-done(((bf16[4,96,2048]{2,1,0:T(8,128)(2,1)}), bf16[4,96,2048]{2,1,0:T(8,128)(2,1)S(1)}, u32[]{:S(2)}, u32[]{:S(2)}) %all-to-all-start.1) | async-done | bytes 1572896 | tf_op jit(solution)/shard_map/all_to_all | solution.py:135
  244.7 2.3 gather_fusion.1
  247.1 2.4 reshape.163
  249.4 3.9 %multiply_reduce_fusion = bf16[128,2048]{1,0:T(8,128)(2,1)} fusion(f32[128,2,2048]{2,1,0:T(2,128)S(1)} %reshape.163, f32[128,2]{1,0:T(8,128)S(1)} %copy.29), kind=kLoop, calls=%fused_computation.42 | loop fusion | flops 786432 | bytes 2622464 | tf_op jit(solution)/shard_map/reduce_sum | solution.py:140
  (95 shorter events, 10.3 us)
Async XLA Ops:
  7.2 72.7 %copy-start = (bf16[2,128,2048]{2,1,0:T(8,128)(2,1)S(1)}, bf16[2,128,2048]{2,1,0:T(8,128)(2,1)}, u32[]{:S(2)}) copy-start(bf16[2,128,2048]{2,1,0:T(8,128)(2,1)} %param.23) | copy-start | bytes 3145732
  7.2 5.6 %copy-start.6 = (s32[128,2]{0,1:T(2,128)S(1)}, s32[128,2]{0,1:T(2,128)}, u32[]{:S(2)}) copy-start(s32[128,2]{0,1:T(2,128)} %param.26) | copy-start | bytes 3076
  7.2 6.0 %copy-start.4 = (bf16[512,2,128]{2,1,0:T(2,128)(2,1)S(1)}, bf16[512,2,128]{2,1,0:T(2,128)(2,1)}, u32[]{:S(2)}) copy-start(bf16[512,2,128]{2,1,0:T(2,128)(2,1)} %param.18) | copy-start | bytes 786436
  7.2 9.5 %copy-start.1 = (bf16[128,2048]{1,0:T(8,128)(2,1)S(1)}, bf16[128,2048]{1,0:T(8,128)(2,1)}, u32[]{:S(2)}) copy-start(bf16[128,2048]{1,0:T(8,128)(2,1)} %param.24) | copy-start | bytes 1572868
  7.2 32.5 %all-gather.6.cloned.1.call-start = ((), (), s32[]{:S(2)}) async-start(), calls=%async_computation.3 | async-start | bytes 1310720 | tf_op jit(solution)/shard_map/all_gather | solution.py:53
  9.1 7.9 %copy-start.5 = (f32[2048]{0:T(1024)S(1)}, f32[2048]{0:T(1024)}, u32[]{:S(2)}) copy-start(f32[2048]{0:T(1024)} %param.25) | copy-start | bytes 24580
  9.1 59.0 %all-gather.8.cloned.1.call-start = ((), (), s32[]{:S(2)}) async-start(), calls=%async_computation.4 | async-start | bytes 1310720 | tf_op jit(solution)/shard_map/all_gather | solution.py:54
  10.8 109.8 %all-gather.10.cloned.1.call-start = ((), (), s32[]{:S(2)}) async-start(), calls=%async_computation.6 | async-start | bytes 4718592 | tf_op jit(solution)/shard_map/all_gather | solution.py:120
  11.6 153.4 %all-gather.12.cloned.1.call-start = ((), (), s32[]{:S(2)}) async-start(), calls=%async_computation.7 | async-start | bytes 4718592 | tf_op jit(solution)/shard_map/all_gather | solution.py:121
  12.2 200.3 %all-gather.14.cloned.1.call-start = ((), (), s32[]{:S(2)}) async-start(), calls=%async_computation.8 | async-start | bytes 4718592 | tf_op jit(solution)/shard_map/all_gather | solution.py:122
  12.7 240.6 %reduce-scatter.2.cloned.1.call-start = ((), (), s32[]{:S(2)}) async-start(), calls=%async_computation.5 | async-start | bytes 2359296 | tf_op jit(solution)/shard_map/reduce_scatter | solution.py:81
  69.5 9.9 %copy-start.8 = (f32[2]{0:T(128)S(1)}, f32[2]{0:T(128)}, u32[]{:S(2)}) copy-start(f32[2]{0:T(128)} %param.21) | copy-start | bytes 28
  69.5 10.4 %copy-start.9 = (f32[128]{0:T(128)S(1)}, f32[128]{0:T(128)}, u32[]{:S(2)}) copy-start(f32[128]{0:T(128)} %param.22) | copy-start | bytes 1540
  79.9 2.2 copy-start.2
  120.7 91.8 %copy-start.3 = (bf16[4,96,2048]{2,1,0:T(8,128)(2,1)S(1)}, bf16[4,96,2048]{2,1,0:T(8,128)(2,1)}, u32[]{:S(2)}) copy-start(bf16[4,96,2048]{2,1,0:T(8,128)(2,1)} %all_to_all.10) | copy-start | bytes 4718596
  221.1 3.8 %copy-start.7 = (f32[128,2]{0,1:T(2,128)S(1)}, f32[128,2]{0,1:T(2,128)}, u32[]{:S(2)}) copy-start(f32[128,2]{0,1:T(2,128)} %param.28) | copy-start | bytes 3076
  221.1 3.8 %copy-start.10 = (f32[128]{0:T(128)S(1)}, f32[128]{0:T(128)}, u32[]{:S(2)}) copy-start(f32[128]{0:T(128)} %param.27) | copy-start | bytes 1540
  221.1 23.6 %all-to-all-start.1 = ((bf16[4,96,2048]{2,1,0:T(8,128)(2,1)}), bf16[4,96,2048]{2,1,0:T(8,128)(2,1)S(1)}, u32[]{:S(2)}, u32[]{:S(2)}) async-start(bf16[4,96,2048]{2,1,0:T(8,128)(2,1)} %bitcast.65), calls=%async_computation.2 | async-start | bytes 3145728 | tf_op jit(solution)/shard_map/all_to_all | solution.py:135
Sparse Core Ops, SparseCore 0:
  10.4 29.2 all-gather.5
  41.5 26.4 all-gather.7
  69.7 47.8 all-gather.9
  119.0 45.9 all-gather.11
  166.4 45.9 all-gather.13
  215.2 34.1 reduce-scatter.1
where the time goes:
time: 261 us; the launch traced here: 260 us
  waiting for transfers between devices  155 us (59%)
  blocking collectives  36.1 us (14%)
  local copies, waits for them, and re-layouts  20.4 us (8%)
  matrix products  19.2 us (7%)
  between operations  14.4 us (6%)
  other arithmetic  7.89 us (3%)
  starting transfers between devices  4.02 us (2%)
  loops' own time  2.93 us (1%)
    all_gather x1, waiting for transfers between devices, expert_half(): piece_down = lax.all_gather(down_weight, 'tp', axis=2, tiled=True)  47.5 us
    all_gather x1, waiting for transfers between devices, expert_half(): piece_up = lax.all_gather(up_weight, 'tp', axis=2, tiled=True)  38.6 us
    all_to_all x1, blocking collectives, expert_half(): lax.all_to_all(outgoing, 'ep', split_axis=0, concat_axis=0, tiled=True)  36.1 us
    all_gather x1, waiting for transfers between devices, attend_heads(): value_piece = lax.all_gather(values, 'ep', axis=0, tiled=True)  26.1 us
    all_gather x1, waiting for transfers between devices, attend_heads(): key_piece = lax.all_gather(keys, 'ep', axis=0, tiled=True)  21.8 us
    all_to_all x1, waiting for transfers between devices, expert_half(): lax.all_to_all(outbound, 'ep', split_axis=0, concat_axis=0, tiled=True)  19.7 us
    dot_general x1, matrix products, expert_half(): jnp.einsum('jrf,jdf->jrd', hidden, piece_down, preferred_element_type=jnp...  8.63 us
    unnamed x28, local copies, waits for them, and re-layouts  7.42 us
  transfers between devices with their start and end apart: 7, of which 5 were waited for; matrix products, arithmetic and copies ran while one was open for 18% of the time, Pallas kernels for 0%

commit v1 on v0

--- a/solution.py
+++ b/solution.py
@@ -5,6 +5,22 @@
 from jax.sharding import PartitionSpec as P
 
 HEAD = 64
+
+
+def summed_both_ways(x, axis, dim, term):
+    devices, index, extent = (lax.axis_size(axis), lax.axis_index(axis), x.shape[dim])
+    right = [(i, (i + 1) % devices) for i in range(devices)]
+    backward = [(i, (i - 1) % devices) for i in range(devices)]
+    half = devices // 2
+    from_left = from_right = x
+    total = term(x, index * extent)
+    for lap in range(1, half + 1):
+        from_left = lax.ppermute(from_left, axis, right)
+        if lap < devices - half:
+            from_right = lax.ppermute(from_right, axis, backward)
+            total = total + term(from_right, (index + lap) % devices * extent)
+        total = total + term(from_left, (index - lap) % devices * extent)
+    return total
 
 
 def attend_heads(queries, keys, values, mixing, head_gain):
@@ -119,14 +135,21 @@
     expert_rows = expert_rows.reshape(local_count, ep_count * capacity, width)
     piece_gate = lax.all_gather(gate_weight, "tp", axis=2, tiled=True)
     piece_up = lax.all_gather(up_weight, "tp", axis=2, tiled=True)
-    piece_down = lax.all_gather(down_weight, "tp", axis=2, tiled=True)
     gate_part = jnp.einsum(
         "jrd,jdf->jrf", expert_rows, piece_gate, preferred_element_type=jnp.float32
     )
     up_part = jnp.einsum("jrd,jdf->jrf", expert_rows, piece_up, preferred_element_type=jnp.float32)
     hidden = (jax.nn.silu(gate_part) * up_part).astype(jnp.bfloat16)
-    expert_out = jnp.einsum(
-        "jrf,jdf->jrd", hidden, piece_down, preferred_element_type=jnp.float32
+    expert_out = summed_both_ways(
+        down_weight,
+        "tp",
+        2,
+        lambda shard, offset_2: jnp.einsum(
+            "jrf,jdf->jrd",
+            lax.dynamic_slice_in_dim(hidden, offset_2, shard.shape[2], axis=2),
+            shard,
+            preferred_element_type=jnp.float32,
+        ),
     ).astype(jnp.bfloat16)
     outbound = jnp.transpose(
         expert_out.reshape(local_count, ep_count, capacity, width), (1, 0, 2, 3)

time: 261 us -> 231 us (0.89)
  blocking collectives: 36.1 us -> 0 us
  starting transfers between devices: 4.02 us -> 21.5 us
  waiting for transfers between devices: 155 us -> 138 us
  matrix products: 19.2 us -> 25.7 us
    all_gather x1 -> x0, waiting for transfers between devices: 47.5 us -> none  [expert_half(): piece_down = lax.all_gather(down_weight, 'tp', axis=2, tiled=True)]
    all_to_all x1 -> x0, blocking collectives: 36.1 us -> none  [expert_half(): lax.all_to_all(outgoing, 'ep', split_axis=0, concat_axis=0, tiled=True)]
    all_gather x1, waiting for transfers between devices: 0.01 us -> 35.2 us  [expert_half(): piece_gate = lax.all_gather(gate_weight, 'tp', axis=2, tiled=True)]
    all_gather x1, waiting for transfers between devices: 21.8 us -> 0.01 us  [attend_heads(): key_piece = lax.all_gather(keys, 'ep', axis=0, tiled=True)]
    ppermute x0 -> x7, waiting for transfers between devices: none -> 13.1 us  [the longest x4 13.1 us: summed_both_ways(): from_left = lax.ppermute(from_left, axis, right)]
    ppermute x0 -> x7, starting transfers between devices: none -> 11.5 us  [the longest x3 11 us: summed_both_ways(): from_right = lax.ppermute(from_right, axis, backward)]
    dot_general x1 -> x9, matrix products: 8.63 us -> 16.4 us  [the longest x8 11.8 us: expert_half(): jnp.einsum('jrf,jdf->jrd', lax.dynamic_slice_in_dim(hidden, offset_2, sha...]
    all_to_all x0 -> x1, starting transfers between devices: none -> 5.85 us  [expert_half(): lax.all_to_all(outgoing, 'ep', split_axis=0, concat_axis=0, tiled=True)]
  transfers between devices with their start and end apart: 7 -> 14, of which waited for: 5 -> 6; matrix products, arithmetic and copies ran while one was open for 18% -> 23% of each run, Pallas kernels for 0% -> 0%
where the time goes in v1:
time: 231 us
  waiting for transfers between devices  138 us (60%)
  matrix products  25.7 us (11%)
  local copies, waits for them, and re-layouts  21.5 us (9%)
  starting transfers between devices  21.5 us (9%)
  between operations  14.3 us (6%)
  other arithmetic  7.09 us (3%)
  loops' own time  3.11 us (1%)
    all_gather x1, waiting for transfers between devices, expert_half(): piece_up = lax.all_gather(up_weight, 'tp', axis=2, tiled=True)  43 us
    all_gather x1, waiting for transfers between devices, expert_half(): piece_gate = lax.all_gather(gate_weight, 'tp', axis=2, tiled=True)  35.2 us
    all_gather x1, waiting for transfers between devices, attend_heads(): value_piece = lax.all_gather(values, 'ep', axis=0, tiled=True)  25.4 us
    all_to_all x1, waiting for transfers between devices, expert_half(): lax.all_to_all(outbound, 'ep', split_axis=0, concat_axis=0, tiled=True)  19.5 us
    ppermute x4, waiting for transfers between devices, summed_both_ways(): from_left = lax.ppermute(from_left, axis, right)  13.1 us
    dot_general x8, matrix products, expert_half(): jnp.einsum('jrf,jdf->jrd', lax.dynamic_slice_in_dim(hidden, offset_2, sha...  11.8 us
    ppermute x3, starting transfers between devices, summed_both_ways(): from_right = lax.ppermute(from_right, axis, backward)  11 us
    unnamed x36, local copies, waits for them, and re-layouts  7.9 us
  transfers between devices with their start and end apart: 14, of which 6 were waited for; matrix products, arithmetic and copies ran while one was open for 23% of the time, Pallas kernels for 0%

profile of v1, /device:TPU:0, one launch (start us, length us, event | category | flops | bytes accessed | tf_op | source)
XLA Modules:
  0.0 230.7 jit_solution(10217454517277534988)
XLA Ops:
  7.3 1.8 copy.24
  9.2 1.7 copy.25
  12.8 4.1 %collective-permute-start = (bf16[1,2048,128]{2,1,0:T(8,128)(2,1)S(1)}, bf16[1,2048,128]{2,1,0:T(8,128)(2,1)S(1)}, u32[]{:S(2)}, u32[]{:S(2)}) collective-permute-start(bf16[1,2048,128]{2,1,0:T(8,128)(2,1)S(1)} %copy-done.2), channel_id=1, source_target_pairs={{0,7},{1,0},{2,1},{3,2},{4,3},{5,4},{6,5},{7,6},{8,15},{9,8},{10,9... | collective-permute-start | bytes 1572872 | tf_op jit(solution)/shard_map/ppermute | solution.py:20
  19.4 7.3 %collective-permute-done.1 = bf16[1,2048,128]{2,1,0:T(8,128)(2,1)S(1)} collective-permute-done((bf16[1,2048,128]{2,1,0:T(8,128)(2,1)S(1)}, bf16[1,2048,128]{2,1,0:T(8,128)(2,1)S(1)}, u32[]{:S(2)}, u32[]{:S(2)}) %collective-permute-start.1) | collective-permute-done | bytes 524320 | tf_op jit(solution)/shard_map/ppermute | solution.py:18
  28.3 3.6 %collective-permute-start.2 = (bf16[1,2048,128]{2,1,0:T(8,128)(2,1)S(1)}, bf16[1,2048,128]{2,1,0:T(8,128)(2,1)}, u32[]{:S(2)}, u32[]{:S(2)}) collective-permute-start(bf16[1,2048,128]{2,1,0:T(8,128)(2,1)S(1)} %collective-permute-done), channel_id=1, source_target_pairs={{0,7},{1,0},{2,1},{3,2},{4,3},{5,4},{6,5},{7,6},{8,15},{9,8},{10,9... | collective-permute-start | bytes 1572872 | tf_op jit(solution)/shard_map/ppermute | solution.py:20
  31.9 5.8 %collective-permute-done.3 = bf16[1,2048,128]{2,1,0:T(8,128)(2,1)} collective-permute-done((bf16[1,2048,128]{2,1,0:T(8,128)(2,1)S(1)}, bf16[1,2048,128]{2,1,0:T(8,128)(2,1)}, u32[]{:S(2)}, u32[]{:S(2)}) %collective-permute-start.3) | collective-permute-done | bytes 524320 | tf_op jit(solution)/shard_map/ppermute | solution.py:18
  37.8 3.1 %gather_fusion = bf16[384,2048]{1,0:T(8,128)(2,1)} fusion(bf16[129,2048]{1,0:T(8,128)(2,1)S(1)} %concatenate.3, s32[1024]{0:T(1024)S(1)} %pad_clamp_fusion.1), kind=kCustom, calls=%fused_computation | custom fusion | bytes 3147264 | tf_op jit(solution)/shard_map/gather | solution.py:130
  40.9 5.8 %all-to-all-start = ((bf16[4,96,2048]{2,1,0:T(8,128)(2,1)}), bf16[4,96,2048]{2,1,0:T(8,128)(2,1)}, u32[]{:S(2)}, u32[]{:S(2)}) async-start(bf16[4,96,2048]{2,1,0:T(8,128)(2,1)} %bitcast.11), calls=%async_computation.1 | async-start | bytes 3145728 | tf_op jit(solution)/shard_map/all_to_all | solution.py:131
  47.0 3.3 %collective-permute-start.4 = (bf16[1,2048,128]{2,1,0:T(8,128)(2,1)}, bf16[1,2048,128]{2,1,0:T(8,128)(2,1)}, u32[]{:S(2)}, u32[]{:S(2)}) collective-permute-start(bf16[1,2048,128]{2,1,0:T(8,128)(2,1)} %collective-permute-done.2), channel_id=1, source_target_pairs={{0,7},{1,0},{2,1},{3,2},{4,3},{5,4},{6,5},{7,6},{8,15},{9,8},{10,9... | collective-permute-start | bytes 1572872 | tf_op jit(solution)/shard_map/ppermute | solution.py:20
  50.3 2.3 copy.26
  52.6 25.4 %all-gather.7.cloned.1.call-done = bf16[2048,2,128]{2,0,1:T(8,128)(2,1)} async-done(((bf16[512,2,128]{2,0,1:T(8,128)(2,1)}), bf16[2048,2,128]{2,0,1:T(8,128)(2,1)}) %all-gather.7.cloned.1.call-update) | async-done | bytes 1048592 | tf_op jit(solution)/shard_map/all_gather | solution.py:70
  79.4 10.0 %while.23 = (s32[]{:T(128)}, f32[2,512]{1,0:T(2,128)S(1)}, f32[2,512]{1,0:T(2,128)S(1)}, f32[2,512,128]{2,1,0:T(8,128)S(1)}, f32[2,512]{1,0:T(2,128)S(1)}, /*ind...) while((s32[]{:T(128)}, f32[2,512]{1,0:T(2,128)S(1)}, ...), condition=%wide.region_7.8_spmd.clone, body=%wide.region_0.7_spmd.clone.sunk | while | flops 410784768 | bytes 17183128 | solution.py:86
  80.7 4.6 %conditional.3 = ((f32[2,512]{1,0:T(2,128)S(1)}, f32[2,512]{1,0:T(2,128)S(1)}, f32[2,512,128]{2,1,0:T(8,128)S(1)}, f32[2,512]{1,0:T(2,128)S(1)}, f32[2,512]{1,0:T(2,128)S(1)}, /*index=5*/f32[2,512,128]{2,1,0:T(8,128)S(1)})) conditional(s32[]{:T(128)} %convert_element_type.85, (f32[2,512]{1,0:T(2,128)S(1)}, f32[2,512]{1,0:T(2,128)S(1)}, ...), branch_computations={%region_1.1_spmd, %region_2.6_spmd} | conditional | flops 410784768 | bytes 17180748 | solution.py:78
  90.0 2.2 bitcast_convert_fusion
  92.2 35.2 %all-gather.9.cloned.1.call-done = bf16[1,2048,1024]{2,1,0:T(8,128)(2,1)} async-done(((bf16[1,2048,128]{2,1,0:T(8,128)(2,1)}), bf16[1,2048,1024]{2,1,0:T(8,128)(2,1)}) %all-gather.9.cloned.1.call-update) | async-done | bytes 4194320 | tf_op jit(solution)/shard_map/all_gather | solution.py:136
  127.4 4.4 %fusion.22 = f32[384,1024]{1,0:T(8,128)S(1)} fusion(bf16[384,2048]{1,0:T(8,128)(2,1)} %bitcast.12, bf16[1,2048,1024]{2,1,0:T(8,128)(2,1)} %all-gather.9.cloned.1.call-done), kind=kOutput, calls=%fused_computation.36 | convolution fusion | flops 1610612736 | bytes 7340032 | tf_op jit(solution)/shard_map/jrd,jdf->jrf/dot_general | solution.py:138
  131.9 43.0 %all-gather.11.cloned.1.call-done = bf16[1,2048,1024]{2,1,0:T(8,128)(2,1)} async-done(((bf16[1,2048,128]{2,1,0:T(8,128)(2,1)}), bf16[1,2048,1024]{2,1,0:T(8,128)(2,1)}) %all-gather.11.cloned.1.call-update) | async-done | bytes 4194320 | tf_op jit(solution)/shard_map/all_gather | solution.py:137
  174.9 4.6 %multiply_convert_fusion = bf16[384,1024]{1,0:T(8,128)(2,1)S(1)} fusion(f32[384,1024]{1,0:T(8,128)S(1)} %fusion.22, bf16[384,2048]{1,0:T(8,128)(2,1)} %bitcast.12, bf16[1,2048,1024]{2,1,0:T(8,128)(2,1)} %all-gather.11.cloned.1.call-done), kind=kOutput, calls=%fused_computation.41 | convolution fusion | flops 1612972032 | bytes 8126464 | tf_op jit(solution)/shard_map/jrd,jdf->jrf/dot_general | solution.py:141
  188.3 3.5 %add_convert_fusion = bf16[384,2048]{1,0:T(8,128)(2,1)} fusion(f32[384,2048]{1,0:T(8,128)S(1)} %fusion.30, f32[384,2048]{1,0:T(8,128)S(1)} %fusion.32, f32[384,2048]{1,0:T(8,128)S(1)} %fusion.34, f32[384,2048]{1,0:T(8,128)S(1)} %fusion.36, f32[384,2048]{1,0:T(8,128)S(1)} %fusion.38, f32[384,2048]{1,0:T(8,128)S(1)} %fusion.42, f32[384,2048]{1,0:T(8,128)S(1)} %fusion.40, ...), kind=kOutput, calls=%fused_computation.39 | convolution fusion | flops 207618048 | bytes 24215556 | tf_op jit(solution)/shard_map/jrf,jdf->jrd/dot_general | solution.py:147
  191.9 3.9 %all-to-all-start.1 = ((bf16[4,96,2048]{2,1,0:T(8,128)(2,1)}), bf16[4,96,2048]{2,1,0:T(8,128)(2,1)S(1)}, u32[]{:S(2)}, u32[]{:S(2)}) async-start(bf16[4,96,2048]{2,1,0:T(8,128)(2,1)} %bitcast.79), calls=%async_computation.2 | async-start | bytes 3145728 | tf_op jit(solution)/shard_map/all_to_all | solution.py:158
  195.9 19.5 %all-to-all-done.1 = bf16[4,96,2048]{2,1,0:T(8,128)(2,1)S(1)} async-done(((bf16[4,96,2048]{2,1,0:T(8,128)(2,1)}), bf16[4,96,2048]{2,1,0:T(8,128)(2,1)S(1)}, u32[]{:S(2)}, u32[]{:S(2)}) %all-to-all-start.1) | async-done | bytes 1572896 | tf_op jit(solution)/shard_map/all_to_all | solution.py:158
  215.5 2.3 %gather_fusion.1 = bf16[256,2048]{1,0:T(8,128)(2,1)} fusion(bf16[384,2048]{1,0:T(8,128)(2,1)S(1)} %bitcast.78, s32[1024]{0:T(1024)S(1)} %pad_clamp_fusion), kind=kCustom, calls=%fused_computation.1 | custom fusion | bytes 2098176 | tf_op jit(solution)/shard_map/gather | solution.py:161
  217.8 2.4 %reshape.227 = f32[128,2,2048]{2,1,0:T(2,128)S(1)} reshape(bf16[256,2048]{1,0:T(8,128)(2,1)} %gather_fusion.1) | data formatting | bytes 3145728 | tf_op jit(solution)/shard_map/convert_element_type | solution.py:161
  220.2 3.9 %multiply_reduce_fusion = bf16[128,2048]{1,0:T(8,128)(2,1)} fusion(f32[128,2,2048]{2,1,0:T(2,128)S(1)} %reshape.227, f32[128,2]{1,0:T(8,128)S(1)} %copy.29), kind=kLoop, calls=%fused_computation.40 | loop fusion | flops 786432 | bytes 2622464 | tf_op jit(solution)/shard_map/reduce_sum | solution.py:163
  (123 shorter events, 24.0 us)
Async XLA Ops:
  7.2 82.8 %copy-start = (bf16[2,128,2048]{2,1,0:T(8,128)(2,1)S(1)}, bf16[2,128,2048]{2,1,0:T(8,128)(2,1)}, u32[]{:S(2)}) copy-start(bf16[2,128,2048]{2,1,0:T(8,128)(2,1)} %param.23) | copy-start | bytes 3145732
  7.2 9.7 %copy-start.10 = (s32[128,2]{0,1:T(2,128)S(1)}, s32[128,2]{0,1:T(2,128)}, u32[]{:S(2)}) copy-start(s32[128,2]{0,1:T(2,128)} %param.26) | copy-start | bytes 3076
  7.2 11.9 %copy-start.1 = (bf16[128,2048]{1,0:T(8,128)(2,1)S(1)}, bf16[128,2048]{1,0:T(8,128)(2,1)}, u32[]{:S(2)}) copy-start(bf16[128,2048]{1,0:T(8,128)(2,1)} %param.24) | copy-start | bytes 1572868
  7.2 20.9 %copy-start.9 = (f32[2048]{0:T(1024)S(1)}, f32[2048]{0:T(1024)}, u32[]{:S(2)}) copy-start(f32[2048]{0:T(1024)} %param.25) | copy-start | bytes 24580
  7.2 43.1 %all-gather.5.cloned.1.call-start = ((), (), s32[]{:S(2)}) async-start(), calls=%async_computation.3 | async-start | bytes 1310720 | tf_op jit(solution)/shard_map/all_gather | solution.py:69
  9.1 68.9 %all-gather.7.cloned.1.call-start = ((), (), s32[]{:S(2)}) async-start(), calls=%async_computation.4 | async-start | bytes 1310720 | tf_op jit(solution)/shard_map/all_gather | solution.py:70
  10.9 116.5 %all-gather.9.cloned.1.call-start = ((), (), s32[]{:S(2)}) async-start(), calls=%async_computation.6 | async-start | bytes 4718592 | tf_op jit(solution)/shard_map/all_gather | solution.py:136
  11.6 163.3 %all-gather.11.cloned.1.call-start = ((), (), s32[]{:S(2)}) async-start(), calls=%async_computation.7 | async-start | bytes 4718592 | tf_op jit(solution)/shard_map/all_gather | solution.py:137
  12.2 14.5 %collective-permute-start.1 = (bf16[1,2048,128]{2,1,0:T(8,128)(2,1)S(1)}, bf16[1,2048,128]{2,1,0:T(8,128)(2,1)S(1)}, u32[]{:S(2)}, u32[]{:S(2)}) collective-permute-start(bf16[1,2048,128]{2,1,0:T(8,128)(2,1)S(1)} %copy-done.2), channel_id=1, source_target_pairs={{0,1},{1,2},{2,3},{3,4},{4,5},{5,6},{6,7},{7,0},{8,9},{9,10},{10,1... | collective-permute-start | bytes 1572872 | tf_op jit(solution)/shard_map/ppermute | solution.py:18
  12.8 15.5 %collective-permute-start = (bf16[1,2048,128]{2,1,0:T(8,128)(2,1)S(1)}, bf16[1,2048,128]{2,1,0:T(8,128)(2,1)S(1)}, u32[]{:S(2)}, u32[]{:S(2)}) collective-permute-start(bf16[1,2048,128]{2,1,0:T(8,128)(2,1)S(1)} %copy-done.2), channel_id=1, source_target_pairs={{0,7},{1,0},{2,1},{3,2},{4,3},{5,4},{6,5},{7,6},{8,15},{9,8},{10,9... | collective-permute-start | bytes 1572872 | tf_op jit(solution)/shard_map/ppermute | solution.py:20
  26.7 14.2 %copy-start.4 = (bf16[1,2048,128]{2,1,0:T(8,128)(2,1)}, bf16[1,2048,128]{2,1,0:T(8,128)(2,1)S(1)}, u32[]{:S(2)}) copy-start(bf16[1,2048,128]{2,1,0:T(8,128)(2,1)S(1)} %collective-permute-done.1) | copy-start | bytes 1572868
  26.7 11.0 %collective-permute-start.3 = (bf16[1,2048,128]{2,1,0:T(8,128)(2,1)S(1)}, bf16[1,2048,128]{2,1,0:T(8,128)(2,1)}, u32[]{:S(2)}, u32[]{:S(2)}) collective-permute-start(bf16[1,2048,128]{2,1,0:T(8,128)(2,1)S(1)} %collective-permute-done.1), channel_id=1, source_target_pairs={{0,1},{1,2},{2,3},{3,4},{4,5},{5,6},{6,7},{7,0},{8,9},{9,10},{10,1... | collective-permute-start | bytes 1572872 | tf_op jit(solution)/shard_map/ppermute | solution.py:18
  28.3 12.6 %copy-start.6 = (bf16[1,2048,128]{2,1,0:T(8,128)(2,1)}, bf16[1,2048,128]{2,1,0:T(8,128)(2,1)S(1)}, u32[]{:S(2)}) copy-start(bf16[1,2048,128]{2,1,0:T(8,128)(2,1)S(1)} %collective-permute-done) | copy-start | bytes 1572868
  28.3 18.7 %collective-permute-start.2 = (bf16[1,2048,128]{2,1,0:T(8,128)(2,1)S(1)}, bf16[1,2048,128]{2,1,0:T(8,128)(2,1)}, u32[]{:S(2)}, u32[]{:S(2)}) collective-permute-start(bf16[1,2048,128]{2,1,0:T(8,128)(2,1)S(1)} %collective-permute-done), channel_id=1, source_target_pairs={{0,7},{1,0},{2,1},{3,2},{4,3},{5,4},{6,5},{7,6},{8,15},{9,8},{10,9... | collective-permute-start | bytes 1572872 | tf_op jit(solution)/shard_map/ppermute | solution.py:20
  37.7 12.6 %collective-permute-start.5 = (bf16[1,2048,128]{2,1,0:T(8,128)(2,1)}, bf16[1,2048,128]{2,1,0:T(8,128)(2,1)}, u32[]{:S(2)}, u32[]{:S(2)}) collective-permute-start(bf16[1,2048,128]{2,1,0:T(8,128)(2,1)} %collective-permute-done.3), channel_id=1, source_target_pairs={{0,1},{1,2},{2,3},{3,4},{4,5},{5,6},{6,7},{7,0},{8,9},{9,10},{10,1... | collective-permute-start | bytes 1572872 | tf_op jit(solution)/shard_map/ppermute | solution.py:18
  40.9 5.9 %copy-start.8 = (bf16[512,2,128]{2,1,0:T(2,128)(2,1)S(1)}, bf16[512,2,128]{2,1,0:T(2,128)(2,1)}, u32[]{:S(2)}) copy-start(bf16[512,2,128]{2,1,0:T(2,128)(2,1)} %param.18) | copy-start | bytes 786436
  40.9 51.3 %all-to-all-start = ((bf16[4,96,2048]{2,1,0:T(8,128)(2,1)}), bf16[4,96,2048]{2,1,0:T(8,128)(2,1)}, u32[]{:S(2)}, u32[]{:S(2)}) async-start(bf16[4,96,2048]{2,1,0:T(8,128)(2,1)} %bitcast.11), calls=%async_computation.1 | async-start | bytes 3145728 | tf_op jit(solution)/shard_map/all_to_all | solution.py:131
  46.8 177.4 %reduce-scatter.2.cloned.1.call-start = ((), (), s32[]{:S(2)}) async-start(), calls=%async_computation.5 | async-start | bytes 2359296 | tf_op jit(solution)/shard_map/reduce_scatter | solution.py:97
  47.0 139.7 %collective-permute-start.4 = (bf16[1,2048,128]{2,1,0:T(8,128)(2,1)}, bf16[1,2048,128]{2,1,0:T(8,128)(2,1)}, u32[]{:S(2)}, u32[]{:S(2)}) collective-permute-start(bf16[1,2048,128]{2,1,0:T(8,128)(2,1)} %collective-permute-done.2), channel_id=1, source_target_pairs={{0,7},{1,0},{2,1},{3,2},{4,3},{5,4},{6,5},{7,6},{8,15},{9,8},{10,9... | collective-permute-start | bytes 1572872 | tf_op jit(solution)/shard_map/ppermute | solution.py:20
  50.3 138.0 %collective-permute-start.6 = (bf16[1,2048,128]{2,1,0:T(8,128)(2,1)}, bf16[1,2048,128]{2,1,0:T(8,128)(2,1)}, u32[]{:S(2)}, u32[]{:S(2)}) collective-permute-start(bf16[1,2048,128]{2,1,0:T(8,128)(2,1)} %collective-permute-done.5), channel_id=1, source_target_pairs={{0,1},{1,2},{2,3},{3,4},{4,5},{5,6},{6,7},{7,0},{8,9},{9,10},{10,1... | collective-permute-start | bytes 1572872 | tf_op jit(solution)/shard_map/ppermute | solution.py:18
  79.4 10.0 %copy-start.12 = (f32[2]{0:T(128)S(1)}, f32[2]{0:T(128)}, u32[]{:S(2)}) copy-start(f32[2]{0:T(128)} %param.21) | copy-start | bytes 28
  79.4 10.6 %copy-start.13 = (f32[128]{0:T(128)S(1)}, f32[128]{0:T(128)}, u32[]{:S(2)}) copy-start(f32[128]{0:T(128)} %param.22) | copy-start | bytes 1540
  131.9 47.6 %copy-start.3 = (bf16[1,2048,128]{2,1,0:T(8,128)(2,1)S(1)}, bf16[1,2048,128]{2,1,0:T(8,128)(2,1)}, u32[]{:S(2)}) copy-start(bf16[1,2048,128]{2,1,0:T(8,128)(2,1)} %param.31) | copy-start | bytes 1572868
  191.9 23.6 %all-to-all-start.1 = ((bf16[4,96,2048]{2,1,0:T(8,128)(2,1)}), bf16[4,96,2048]{2,1,0:T(8,128)(2,1)S(1)}, u32[]{:S(2)}, u32[]{:S(2)}) async-start(bf16[4,96,2048]{2,1,0:T(8,128)(2,1)} %bitcast.79), calls=%async_computation.2 | async-start | bytes 3145728 | tf_op jit(solution)/shard_map/all_to_all | solution.py:158
  (5 other events, 15.6 us)
Sparse Core Ops, SparseCore 0:
  10.5 29.2 all-gather.4
  41.6 36.3 all-gather.6
  79.6 47.8 all-gather.8
  128.9 46.0 all-gather.10
  177.6 34.1 reduce-scatter.1
